TPU v7x, 512 devices: a whole 4x8x8 slice. The times are simulated.
512 devices in a mesh: sp: 128 (over z, y, core), tp: 4 (over x).
Axes of the slice: x: 4, y: 8, z: 8, core: 2. Of those that a mesh axis runs over, the one named last changes fastest.
Arguments:
- tokens: bfloat16 [65536, 2048], P('sp'), may hold values from -6 to 6
- norm_gain: bfloat16 [2048], replicated, may hold values from 0.099609375 to 1.8984375
- w_conv_value: bfloat16 [2048, 2048], P('sp', 'tp'), may hold values from -0.125 to 0.125
- w_conv_gate: bfloat16 [2048, 2048], P('sp', 'tp'), may hold values from -0.125 to 0.125
- w_query: bfloat16 [2048, 2048], P('sp', 'tp'), may hold values from -0.125 to 0.125
- w_key: bfloat16 [2048, 512], P('sp', 'tp'), may hold values from -0.125 to 0.125
- w_value: bfloat16 [2048, 512], P('sp', 'tp'), may hold values from -0.125 to 0.125
- conv_taps: float32 [31, 2048], P(None, 'tp'), as said below
- ln_gain: float32 [2048], P('tp'), may hold values from 0.1 to 1.9
- sinks: float32 [32], P('tp'), may hold values from 3 to 6
- out_conv: bfloat16 [2048, 2048], P('tp', 'sp'), may hold values from -0.125 to 0.125
- out_attn: bfloat16 [2048, 2048], P('tp', 'sp'), may hold values from -0.5 to 0.5
Outputs:
- mixed: bfloat16 [65536, 2048], P(('sp', 'tp'))
- log_sums: float32 [32, 65536], P('tp', 'sp')
Inputs may be any that keep to these rules, and one draw needn't show every extreme that they name: `conv_taps`: each tap lies within 30 / sqrt(31) in magnitude.
All inputs are finite; a program needn't handle non-finite values.
Results may differ from a plain program's by a relative error of at most 0.017.
Values may be sent and summed in bfloat16 or wider, within the bound.
A program may use at most 64 MiB of HBM per device.

v0:
```python
import jax
import jax.numpy as jnp
from jax import lax
from jax.sharding import PartitionSpec as P

CONV_CH = 2048
HEADS = 32
KV_HEADS = 8
HEAD_DIM = 64
WINDOW = 128
NORM_EPS = 1e-06
CHANNEL_EPS = 1e-05
ROPE_BASE = 10000.0


def sent_together(arrays, axis, dim, along):
    widths = [a.shape[along] for a in arrays]
    both = jnp.concatenate(arrays, axis=along)
    whole = lax.all_gather(both, axis, axis=dim, tiled=True)
    return tuple(jnp.split(whole, [sum(widths[:k]) for k in range(1, len(widths))], axis=along))


def shifted(value, axis, steps):
    count = lax.axis_size(axis)
    initial, last = (max(0, -steps), min(count, count - steps))
    return lax.ppermute(value, axis, [(source, source + steps) for source in range(initial, last)])


def from_everyone(shard, axis):
    peers = lax.axis_size(axis)
    return lax.all_to_all(
        jnp.broadcast_to(shard[None], (peers, *shard.shape)), axis, 0, 0, tiled=True
    )


def taken_together(shard, axis):
    everything = from_everyone(shard, axis)
    return jnp.sum(everything, axis=0)


def packed_total(arrays, axis):
    ravelled, at, finished = (jnp.concatenate([a.reshape(-1) for a in arrays]), 0, [])
    subtotal = taken_together(ravelled, axis)
    for a in arrays:
        finished.append(subtotal[at : at + a.size].reshape(a.shape))
        at += a.size
    return tuple(finished)


def turned_gather(arrays, axis, dims):
    turned = [jnp.moveaxis(a, dim, 0) for a, dim in zip(arrays, dims)]
    both = jnp.concatenate([t.reshape(len(t), -1) for t in turned], axis=1)
    whole, at, finished = (lax.all_gather(both, axis, axis=0, tiled=True), 0, [])
    for t, dim in zip(turned, dims):
        piece = whole[:, at : at + t[0].size].reshape(-1, *t.shape[1:])
        finished.append(jnp.moveaxis(piece, 0, dim))
        at += t[0].size
    return tuple(finished)


def cut_along(shard, dim, peers):
    dims = shard.shape
    pieces = shard.reshape(*dims[:dim], peers, dims[dim] // peers, *dims[dim + 1 :])
    return jnp.moveaxis(pieces, dim, 0)


def summed_on_arrival(shard, axis, dim):
    pieces = cut_along(shard, dim, lax.axis_size(axis))
    arrived = lax.all_to_all(pieces, axis, split_axis=0, concat_axis=0, tiled=True)
    return arrived.astype(jnp.float32).sum(axis=0)


def rotate(heads, positions):
    half_dim = heads.shape[-1] // 2
    inverse = ROPE_BASE ** (-jnp.arange(half_dim, dtype=jnp.float32) / half_dim)
    angles = positions.astype(jnp.float32)[:, None] * inverse[None, :]
    cosine = jnp.cos(angles)[:, None, :]
    sine = jnp.sin(angles)[:, None, :]
    as_float = heads.astype(jnp.float32)
    front_part = as_float[..., :half_dim]
    back_part = as_float[..., half_dim:]
    return jnp.concatenate(
        [front_part * cosine - back_part * sine, back_part * cosine + front_part * sine], axis=-1
    )


def shards(
    tokens,
    norm_gain,
    w_conv_value,
    w_conv_gate,
    w_query,
    w_key,
    w_value,
    conv_taps,
    ln_gain,
    sinks,
    out_conv,
    out_attn,
):
    as_float = tokens.astype(jnp.float32)
    normed = (
        as_float
        * lax.rsqrt(jnp.mean(as_float * as_float, axis=-1, keepdims=True) + NORM_EPS)
        * norm_gain.astype(jnp.float32)
    ).astype(jnp.bfloat16)
    row_count = normed.shape[0]
    pieces = sent_together((w_conv_value, w_conv_gate, w_query, w_key, w_value), "sp", 0, 1)
    projected = tuple(
        (jnp.dot(normed, piece, preferred_element_type=jnp.float32) for piece in pieces)
    )
    conv_value, conv_gate, query_raw, key_raw, value_rows = [
        item.astype(jnp.bfloat16) for item in projected
    ]
    glu = (conv_value.astype(jnp.float32) * jax.nn.sigmoid(conv_gate.astype(jnp.float32))).astype(
        jnp.bfloat16
    )
    offset = lax.axis_index("sp") * row_count
    positions = offset + jnp.arange(row_count, dtype=jnp.int32)
    query_heads = query_raw.shape[1] // HEAD_DIM
    key_heads = key_raw.shape[1] // HEAD_DIM
    query = rotate(query_raw.reshape(row_count, query_heads, HEAD_DIM), positions).astype(
        jnp.bfloat16
    )
    key = rotate(key_raw.reshape(row_count, key_heads, HEAD_DIM), positions).astype(jnp.bfloat16)
    reach = conv_taps.shape[0] - 1
    key_tail = key[row_count - WINDOW :]
    value_tail = value_rows.reshape(row_count, key_heads, HEAD_DIM)[row_count - WINDOW :]
    glu_tail = glu[row_count - reach :]
    glu_before = shifted(glu_tail, "sp", 1)
    key_before, value_before = shifted((key_tail, value_tail), "sp", 1)
    extended = jnp.concatenate([glu_before, glu], axis=0).astype(jnp.float32)
    conv_out = jnp.zeros((row_count, glu.shape[1]), jnp.float32)
    for tap in range(reach + 1):
        conv_out = conv_out + conv_taps[tap][None, :] * extended[tap : tap + row_count]
    sum_first = jnp.sum(conv_out, axis=-1)
    sum_second = jnp.sum(conv_out * conv_out, axis=-1)
    total_first, total_second = packed_total((sum_first, sum_second), "tp")
    mean = (total_first / CONV_CH)[:, None]
    var = (total_second / CONV_CH)[:, None] - mean * mean
    conv_branch = jax.nn.silu(
        (conv_out - mean) * lax.rsqrt(var + CHANNEL_EPS) * ln_gain[None, :]
    ).astype(jnp.bfloat16)
    group = HEADS // KV_HEADS
    blocks = row_count // WINDOW
    q_blocks = query.reshape(blocks, WINDOW, key_heads, group, HEAD_DIM)
    key_blocks = jnp.concatenate([key_before, key], axis=0).reshape(
        blocks + 1, WINDOW, key_heads, HEAD_DIM
    )
    value_all = jnp.concatenate(
        [value_before, value_rows.reshape(row_count, key_heads, HEAD_DIM)], axis=0
    )
    value_blocks = value_all.reshape(blocks + 1, WINDOW, key_heads, HEAD_DIM)
    key_window = jnp.concatenate([key_blocks[:-1], key_blocks[1:]], axis=1)
    value_window = jnp.concatenate([value_blocks[:-1], value_blocks[1:]], axis=1)
    scores = jnp.einsum(
        "nqhgd,nkhd->nhgqk", q_blocks, key_window, preferred_element_type=jnp.float32
    ) * HEAD_DIM ** (-0.5)
    query_index = jnp.arange(WINDOW)[:, None] + WINDOW
    key_index = jnp.arange(2 * WINDOW)[None, :]
    band = (key_index <= query_index) & (query_index - key_index < WINDOW)
    block_index = jnp.arange(blocks)[:, None, None]
    allowed = band[None] & (offset + block_index * WINDOW + key_index[None] - WINDOW >= 0)
    allowed = allowed[:, None, None]
    totals = jnp.sum(jnp.where(allowed, jnp.exp(scores), 0.0), axis=-1)
    totals = totals + jnp.exp(sinks).reshape(1, key_heads, group, 1)
    log_total = jnp.log(totals)
    weights = jnp.where(allowed, jnp.exp(scores - log_total[..., None]), 0.0).astype(jnp.bfloat16)
    attended = jnp.einsum(
        "nhgqk,nkhd->nqhgd", weights, value_window, preferred_element_type=jnp.float32
    )
    attn_branch = attended.astype(jnp.bfloat16).reshape(row_count, query_heads * HEAD_DIM)
    log_sums = log_total.transpose(1, 2, 0, 3).reshape(query_heads, row_count)
    cols_conv, cols_attn = turned_gather((out_conv, out_attn), "sp", (1, 1))
    mixed = summed_on_arrival(
        (
            jnp.dot(conv_branch, cols_conv, preferred_element_type=jnp.float32)
            + jnp.dot(attn_branch, cols_attn, preferred_element_type=jnp.float32)
        ).astype(jnp.bfloat16),
        "tp",
        0,
    )
    return (mixed.astype(jnp.bfloat16), log_sums)


def solution(mesh):
    in_specs = (
        P("sp", None),
        P(),
        P("sp", "tp"),
        P("sp", "tp"),
        P("sp", "tp"),
        P("sp", "tp"),
        P("sp", "tp"),
        P(None, "tp"),
        P("tp"),
        P("tp"),
        P("tp", "sp"),
        P("tp", "sp"),
    )
    out_specs = (P(("sp", "tp"), None), P("tp", "sp"))
    return jax.shard_map(shards, mesh=mesh, in_specs=in_specs, out_specs=out_specs, check_vma=False)
```

profile of v0, /device:TPU:1, one launch (start us, length us, event | category | flops | bytes accessed | tf_op | source)
XLA Modules:
  0.0 231.2 jit_solution(13513248119261540660)
XLA Ops:
  7.2 0.9 constant_dynamic-update-slice_fusion.4
  11.6 1.3 pad_maximum_fusion.4
  15.1 2.1 fusion
  17.2 1.0 fusion.126
  18.2 1.7 fusion.125
  20.5 84.2 %all-gather.3.cloned.1.call-done = bf16[2048,1792]{1,0:T(8,128)(2,1)} async-done(((bf16[16,1792]{1,0:T(8,128)(2,1)}), bf16[2048,1792]{1,0:T(8,128)(2,1)}) %all-gather.3.cloned.1.call-update) | async-done | bytes 7340048 | tf_op jit(solution)/shard_map/all_gather | solution.py:19
  104.7 2.6 %convolution_convert_fusion.1 = bf16[512,128]{0,1:T(8,128)(2,1)S(1)} fusion(bf16[2048,1792]{1,0:T(8,128)(2,1)} %all-gather.3.cloned.1.call-done, bf16[512,2048]{1,0:T(8,128)(2,1)} %param.12, f32[2048]{0:T(1024)S(1)} %convert_element_type.78, f32[512]{0:T(512)S(1)} %add_rsqrt_fusion.1), kind=kOutput, calls=%fused_computation.41 | convolution fusion | flops 272695296 | bytes 2762752 | tf_op jit(solution)/shard_map/dot_general | solution.py:110
  107.4 2.1 convolution_convert_fusion
  109.6 3.0 %collective-permute-start.2 = (bf16[128,2,64]{0,2,1:T(8,128)(2,1)S(1)}, bf16[128,2,64]{0,2,1:T(8,128)(2,1)S(1)}, u32[]{:S(2)}, u32[]{:S(2)}) collective-permute-start(bf16[128,2,64]{0,2,1:T(8,128)(2,1)S(1)} %pad_maximum_fusion.3), channel_id=1, source_target_pairs={{0,4},{4,8},{8,12},{12,16},{16,20},{20,24},{24,28},{28,32},{32,36}... | collective-permute-start | bytes 98312 | tf_op jit(solution)/shard_map/ppermute | solution.py:26
  112.6 3.0 %fusion.47 = bf16[512,512]{0,1:T(8,128)(2,1)S(1)} fusion(bf16[2048,1792]{1,0:T(8,128)(2,1)} %all-gather.3.cloned.1.call-done, bf16[512,2048]{1,0:T(8,128)(2,1)S(1)} %copy-done, f32[2048]{0:T(1024)S(1)} %convert_element_type.78, f32[512]{0:T(512)S(1)} %add_rsqrt_fusion.1), kind=kOutput, calls=%fused_computation.35 | convolution fusion | flops 1078198272 | bytes 4728832 | tf_op jit(solution)/shard_map/dot_general | solution.py:110
  115.7 1.5 fusion.56
  117.2 1.3 fusion.50
  118.5 2.1 collective-permute-start
  121.1 3.7 %collective-permute-start.1 = (bf16[128,2,64]{0,2,1:T(8,128)(2,1)S(1)}, bf16[128,2,64]{0,2,1:T(8,128)(2,1)S(1)}, u32[]{:S(2)}, u32[]{:S(2)}) collective-permute-start(bf16[128,2,64]{0,2,1:T(8,128)(2,1)S(1)} %bitcast.113), channel_id=1, source_target_pairs={{0,4},{4,8},{8,12},{12,16},{16,20},{20,24},{24,28},{28,32},{32,36}... | collective-permute-start | bytes 98312 | tf_op jit(solution)/shard_map/ppermute | solution.py:26
  125.1 5.1 %fusion.123 = (f32[512]{0:T(512)S(1)}, f32[512]{0:T(512)S(1)}, f32[512,512]{1,0:T(8,128)S(1)}) fusion(f32[542,512]{1,0:T(8,128)S(1)} %maximum_convert_fusion, f32[512]{0:T(512)S(1)} %bitcast.127, f32[512]{0:T(512)S(1)} %bitcast.128, f32[512]{0:T(512)S(1)} %bitcast.130, f32[512]{0:T(512)S(1)} %bitcast.131, f32[512]{0:T(512)S(1)} %bitcast.132, ...), kind=kLoop, calls=%fused_computation.167 | loop fusion | flops 16776192 | bytes 33622016 | tf_op jit(solution)/shard_map/reduce_sum | solution.py:136
  130.8 4.0 %all-to-all-start = ((f32[4,1,1024]{2,1,0:T(1,128)}), f32[4,1,1024]{2,1,0:T(1,128)S(1)}, u32[]{:S(2)}, u32[]{:S(2)}) async-start(f32[4,1,1024]{2,1,0:T(1,128)} %broadcast_in_dim.14), calls=%async_computation | async-start | bytes 32768 | tf_op jit(solution)/shard_map/all_to_all | solution.py:31
  134.8 1.1 fusion.4
  136.1 0.9 fusion.59
  137.4 1.6 all-to-all-done
  139.0 49.8 %all-gather.5.cloned.1.call-done = bf16[2048,1024]{1,0:T(8,128)(2,1)} async-done(((bf16[16,1024]{1,0:T(8,128)(2,1)}), bf16[2048,1024]{1,0:T(8,128)(2,1)}) %all-gather.5.cloned.1.call-update) | async-done | bytes 4194320 | tf_op jit(solution)/shard_map/all_gather | solution.py:53
  188.9 3.2 %fusion.13 = f32[512,2048]{1,0:T(8,128)S(1)} fusion(bf16[2048,1024]{1,0:T(8,128)(2,1)} %all-gather.5.cloned.1.call-done, f32[512,512]{1,0:T(8,128)S(1)} %get-tuple-element.4, f32[512]{0:T(512)S(1)} %copy-done.8, f32[512]{0:T(512)S(1)} %get-tuple-element.41, f32[512]{0:T(512)S(1)} %get-tuple-element.40), kind=kOutput, calls=%fused_computation.17 | convolution fusion | flops 1075838976 | bytes 7346176 | tf_op jit(solution)/shard_map/dot_general | solution.py:177
  192.1 1.3 add_convert_fusion
  193.4 29.6 %all_to_all.11 = bf16[4,128,2048]{2,1,0:T(8,128)(2,1)S(1)} all-to-all(bf16[4,128,2048]{2,1,0:T(8,128)(2,1)S(1)} %bitcast.108), channel_id=1, replica_groups=mesh['sp'=128,'tp'=4] {'tp'}, dimensions={0} | all-to-all | bytes 4194304 | tf_op jit(solution)/shard_map/all_to_all | solution.py:69
  223.0 1.3 reduce_sum.62
  (69 shorter events, 8.3 us)
Async XLA Ops:
  7.2 100.2 %copy-start = (bf16[512,2048]{1,0:T(8,128)(2,1)S(1)}, bf16[512,2048]{1,0:T(8,128)(2,1)}, u32[]{:S(2)}) copy-start(bf16[512,2048]{1,0:T(8,128)(2,1)} %param.12) | copy-start | bytes 6291460
  7.2 97.5 %all-gather.3.cloned.1.call-start = ((), (), s32[]{:S(2)}) async-start(), calls=%async_computation.2 | async-start | bytes 7397376 | tf_op jit(solution)/shard_map/all_gather | solution.py:19
  10.9 0.6 copy-start.2
  11.6 177.3 %all-gather.5.cloned.1.call-start = ((), (), s32[]{:S(2)}) async-start(), calls=%async_computation.3 | async-start | bytes 4227072 | tf_op jit(solution)/shard_map/all_gather | solution.py:53
  107.3 8.3 %slice-start = ((s8[7340032]{0:T(1024)(128)(4,1)}), s8[4194304]{0:T(1024)(128)(4,1)S(1)}, s32[]{:S(2)}) async-start(s8[7340032]{0:T(1024)(128)(4,1)} %bitcast.148), calls=%async_computation.4 | async-start | bytes 8388608
  109.5 6.1 %slice-start.1 = ((s8[7340032]{0:T(1024)(128)(4,1)}), s8[3145728]{0:T(1024)(128)(4,1)S(1)}, s32[]{:S(2)}) async-start(s8[7340032]{0:T(1024)(128)(4,1)} %bitcast.148), calls=%async_computation.5 | async-start | bytes 6291456
  109.6 25.2 %collective-permute-start.2 = (bf16[128,2,64]{0,2,1:T(8,128)(2,1)S(1)}, bf16[128,2,64]{0,2,1:T(8,128)(2,1)S(1)}, u32[]{:S(2)}, u32[]{:S(2)}) collective-permute-start(bf16[128,2,64]{0,2,1:T(8,128)(2,1)S(1)} %pad_maximum_fusion.3), channel_id=1, source_target_pairs={{0,4},{4,8},{8,12},{12,16},{16,20},{20,24},{24,28},{28,32},{32,36}... | collective-permute-start | bytes 98312 | tf_op jit(solution)/shard_map/ppermute | solution.py:26
  118.5 6.6 %copy-start.4 = (f32[1,512]{1,0:T(1,128)S(1)}, f32[1,512]{1,0:T(1,128)}, u32[]{:S(2)}) copy-start(f32[1,512]{1,0:T(1,128)} %get-tuple-element.25) | copy-start | bytes 6148
  118.5 6.6 %copy-start.5 = (f32[1,512]{1,0:T(1,128)S(1)}, f32[1,512]{1,0:T(1,128)}, u32[]{:S(2)}) copy-start(f32[1,512]{1,0:T(1,128)} %get-tuple-element.26) | copy-start | bytes 6148
  118.5 6.6 %copy-start.6 = (f32[1,512]{1,0:T(1,128)S(1)}, f32[1,512]{1,0:T(1,128)}, u32[]{:S(2)}) copy-start(f32[1,512]{1,0:T(1,128)} %get-tuple-element.27) | copy-start | bytes 6148
  118.5 6.3 %collective-permute-start = (bf16[30,512]{1,0:T(8,128)(2,1)S(1)}, bf16[30,512]{1,0:T(8,128)(2,1)S(1)}, u32[]{:S(2)}, u32[]{:S(2)}) collective-permute-start(bf16[30,512]{1,0:T(8,128)(2,1)S(1)} %slice.319), channel_id=1, source_target_pairs={{0,4},{4,8},{8,12},{12,16},{16,20},{20,24},{24,28},{28,32},{32,36}... | collective-permute-start | bytes 92168 | tf_op jit(solution)/shard_map/ppermute | solution.py:26
  121.1 13.7 %collective-permute-start.1 = (bf16[128,2,64]{0,2,1:T(8,128)(2,1)S(1)}, bf16[128,2,64]{0,2,1:T(8,128)(2,1)S(1)}, u32[]{:S(2)}, u32[]{:S(2)}) collective-permute-start(bf16[128,2,64]{0,2,1:T(8,128)(2,1)S(1)} %bitcast.113), channel_id=1, source_target_pairs={{0,4},{4,8},{8,12},{12,16},{16,20},{20,24},{24,28},{28,32},{32,36}... | collective-permute-start | bytes 98312 | tf_op jit(solution)/shard_map/ppermute | solution.py:26
  130.2 5.8 %copy-start.7 = (f32[2,4]{1,0:T(2,128)S(1)}, f32[2,4]{1,0:T(2,128)}, u32[]{:S(2)}) copy-start(f32[2,4]{1,0:T(2,128)} %add.243) | copy-start | bytes 100
  130.8 8.2 %all-to-all-start = ((f32[4,1,1024]{2,1,0:T(1,128)}), f32[4,1,1024]{2,1,0:T(1,128)S(1)}, u32[]{:S(2)}, u32[]{:S(2)}) async-start(f32[4,1,1024]{2,1,0:T(1,128)} %broadcast_in_dim.14), calls=%async_computation | async-start | bytes 32768 | tf_op jit(solution)/shard_map/all_to_all | solution.py:31
  135.9 52.9 %copy-start.8 = (f32[512]{0:T(512)S(1)}, f32[512]{0:T(512)}, u32[]{:S(2)}) copy-start(f32[512]{0:T(512)} %param.20) | copy-start | bytes 6148
  136.1 56.0 %copy-start.3 = (f32[4,2,4,128]{3,2,1,0:T(4,128)}, f32[4,2,4,128]{3,2,1,0:T(4,128)S(1)}, u32[]{:S(2)}) copy-start(f32[4,2,4,128]{3,2,1,0:T(4,128)S(1)} %add_log_fusion) | copy-start | bytes 49156
  188.9 3.2 %copy-start.1 = (bf16[2048,1024]{1,0:T(8,128)(2,1)S(1)}, bf16[2048,1024]{1,0:T(8,128)(2,1)}, u32[]{:S(2)}) copy-start(bf16[2048,1024]{1,0:T(8,128)(2,1)} %all-gather.5.cloned.1.call-done) | copy-start | bytes 12582916
Sparse Core Ops, SparseCore 0:
  11.7 92.9 all-gather.2
  107.8 80.9 all-gather.4
where the time goes:
time: 232 us; the launch traced here: 231 us
  waiting for transfers between devices  136 us (59%)
  blocking collectives  29.6 us (13%)
  matrix products  16.9 us (7%)
  between operations  14.5 us (6%)
  starting transfers between devices  12.9 us (6%)
  other arithmetic  11.8 us (5%)
  local copies, waits for them, and re-layouts  9.71 us (4%)
    all_gather x1, waiting for transfers between devices, sent_together(): whole = lax.all_gather(both, axis, axis=dim, tiled=True)  84.2 us
    all_gather x1, waiting for transfers between devices, turned_gather(): lax.all_gather(both, axis, axis=0, tiled=True)  49.8 us
    all_to_all x1, blocking collectives, summed_on_arrival(): lax.all_to_all(pieces, axis, split_axis=0, concat_axis=0, tiled=True)  29.6 us
    dot_general x5, matrix products, shards(): jnp.dot(normed, piece, preferred_element_type=jnp.float32)  10.4 us
    ppermute x3, starting transfers between devices, shifted(): lax.ppermute(value, axis, [(source, source + steps) for source in range(i...  8.87 us
    reduce_sum x1, other arithmetic, shards(): sum_first = jnp.sum(conv_out, axis=-1)  5.05 us
  transfers between devices with their start and end apart: 6, of which 3 were waited for; matrix products, arithmetic and copies ran while one was open for 12% of the time, Pallas kernels for 0%

commit v1 on v0

--- a/solution.py
+++ b/solution.py
@@ -50,7 +50,13 @@
 def turned_gather(arrays, axis, dims):
     turned = [jnp.moveaxis(a, dim, 0) for a, dim in zip(arrays, dims)]
     both = jnp.concatenate([t.reshape(len(t), -1) for t in turned], axis=1)
-    whole, at, finished = (lax.all_gather(both, axis, axis=0, tiled=True), 0, [])
+    whole, at, finished = (
+        jnp.concatenate(
+            lax.all_to_all(jnp.stack([both] * lax.axis_size(axis)), axis, 0, 0), axis=0
+        ),
+        0,
+        [],
+    )
     for t, dim in zip(turned, dims):
         piece = whole[:, at : at + t[0].size].reshape(-1, *t.shape[1:])
         finished.append(jnp.moveaxis(piece, 0, dim))

time: 232 us -> 291 us (1.25)
  the two profiles are of different devices: /device:TPU:1 before, /device:TPU:32 now
where the time goes in v1:
time: 291 us; the launch traced here: 290 us
  waiting for transfers between devices  174 us (60%)
  blocking collectives  29.1 us (10%)
  starting transfers between devices  22.6 us (8%)
  matrix products  22.3 us (8%)
  between operations  14.4 us (5%)
  other arithmetic  14.1 us (5%)
  local copies, waits for them, and re-layouts  13.4 us (5%)
    all_gather x1, waiting for transfers between devices, sent_together(): whole = lax.all_gather(both, axis, axis=dim, tiled=True)  86.2 us
    ppermute x3, waiting for transfers between devices, shifted(): lax.ppermute(value, axis, [(source, source + steps) for source in range(i...  75.7 us
    all_to_all x1, blocking collectives, summed_on_arrival(): lax.all_to_all(pieces, axis, split_axis=0, concat_axis=0, tiled=True)  29.1 us
    dot_general x5, matrix products, shards(): jnp.dot(normed, piece, preferred_element_type=jnp.float32)  13.4 us
    all_to_all x1, starting transfers between devices, turned_gather(): lax.all_to_all(jnp.stack([both] * lax.axis_size(axis)), axis, 0, 0)  11.5 us
    ppermute x3, starting transfers between devices, shifted(): lax.ppermute(value, axis, [(source, source + steps) for source in range(i...  6.81 us
    all_to_all x1, waiting for transfers between devices, turned_gather(): lax.all_to_all(jnp.stack([both] * lax.axis_size(axis)), axis, 0, 0)  6.62 us
  transfers between devices with their start and end apart: 6, of which 5 were waited for; matrix products, arithmetic and copies ran while one was open for 8% of the time, Pallas kernels for 0%

profile of v1, /device:TPU:32, one launch (start us, length us, event | category | flops | bytes accessed | tf_op | source)
XLA Modules:
  0.0 289.7 jit_solution(15958793626473537208)
XLA Ops:
  12.1 2.1 fusion
  14.2 1.2 fusion.125
  15.4 86.2 %all-gather.2.cloned.1.call-done = bf16[2048,1792]{1,0:T(8,128)(2,1)} async-done(((bf16[16,1792]{1,0:T(8,128)(2,1)}), bf16[2048,1792]{1,0:T(8,128)(2,1)}) %all-gather.2.cloned.1.call-update) | async-done | bytes 7340048 | tf_op jit(solution)/shard_map/all_gather | solution.py:19
  101.6 3.7 %fusion.56 = f32[512,512]{1,0:T(8,128)S(1)} fusion(bf16[2048,1792]{1,0:T(8,128)(2,1)} %all-gather.2.cloned.1.call-done, bf16[512,2048]{1,0:T(8,128)(2,1)} %param.12, f32[2048]{0:T(1024)S(1)} %convert_element_type.78, f32[512]{0:T(512)S(1)} %add_rsqrt_fusion.1), kind=kOutput, calls=%fused_computation.38 | convolution fusion | flops 1079246848 | bytes 5253120 | tf_op jit(solution)/shard_map/dot_general | solution.py:116
  105.3 2.9 fusion.50
  108.2 2.1 collective-permute-start
  111.3 3.3 %collective-permute-done = bf16[30,512]{1,0:T(8,128)(2,1)S(1)} collective-permute-done((bf16[30,512]{1,0:T(8,128)(2,1)S(1)}, bf16[30,512]{1,0:T(8,128)(2,1)S(1)}, u32[]{:S(2)}, u32[]{:S(2)}) %collective-permute-start) | collective-permute-done | bytes 30752 | tf_op jit(solution)/shard_map/ppermute | solution.py:26
  114.8 5.0 %fusion.123 = (f32[512]{0:T(512)S(1)}, f32[512]{0:T(512)S(1)}, f32[512,512]{1,0:T(8,128)S(1)}) fusion(f32[542,512]{1,0:T(8,128)S(1)} %maximum_convert_fusion, f32[512]{0:T(512)S(1)} %bitcast.147, f32[512]{0:T(512)S(1)} %bitcast.148, f32[512]{0:T(512)S(1)} %bitcast.119, f32[512]{0:T(512)S(1)} %bitcast.120, f32[512]{0:T(512)S(1)} %bitcast.121, ...), kind=kLoop, calls=%fused_computation.167 | loop fusion | flops 16776192 | bytes 33622016 | tf_op jit(solution)/shard_map/reduce_sum | solution.py:142
  120.5 4.3 %all-to-all-start = ((f32[4,1,1024]{2,1,0:T(1,128)}), f32[4,1,1024]{2,1,0:T(1,128)S(1)}, u32[]{:S(2)}, u32[]{:S(2)}) async-start(f32[4,1,1024]{2,1,0:T(1,128)} %broadcast_in_dim.14), calls=%async_computation | async-start | bytes 32768 | tf_op jit(solution)/shard_map/all_to_all | solution.py:31
  124.8 5.3 %all-to-all-done = f32[4,1,1024]{2,1,0:T(1,128)S(1)} async-done(((f32[4,1,1024]{2,1,0:T(1,128)}), f32[4,1,1024]{2,1,0:T(1,128)S(1)}, u32[]{:S(2)}, u32[]{:S(2)}) %all-to-all-start) | async-done | bytes 16416 | tf_op jit(solution)/shard_map/all_to_all | solution.py:31
  130.1 2.6 stack.2
  132.7 11.5 %all-to-all-start.1 = ((bf16[128,16,1024]{2,1,0:T(8,128)(2,1)}), bf16[128,16,1024]{2,1,0:T(8,128)(2,1)}, u32[]{:S(2)}, u32[]{:S(2)}) async-start(bf16[128,16,1024]{2,1,0:T(8,128)(2,1)} %stack.2), calls=%async_computation.1 | async-start | bytes 8388608 | tf_op jit(solution)/shard_map/all_to_all | solution.py:55
  146.1 1.9 convolution_convert_fusion
  148.8 2.2 collective-permute-start.2
  151.0 3.0 %fusion.47 = bf16[512,512]{0,1:T(8,128)(2,1)S(1)} fusion(bf16[2048,1792]{1,0:T(8,128)(2,1)} %all-gather.2.cloned.1.call-done, bf16[512,2048]{1,0:T(8,128)(2,1)S(1)} %copy-done, f32[2048]{0:T(1024)S(1)} %convert_element_type.78, f32[512]{0:T(512)S(1)} %add_rsqrt_fusion.1), kind=kOutput, calls=%fused_computation.35 | convolution fusion | flops 1078198272 | bytes 4728832 | tf_op jit(solution)/shard_map/dot_general | solution.py:116
  155.0 1.9 convolution_convert_fusion.1
  158.5 2.5 collective-permute-start.1
  162.2 72.4 %collective-permute-done.2 = bf16[128,2,64]{0,2,1:T(8,128)(2,1)} collective-permute-done((bf16[128,2,64]{0,2,1:T(8,128)(2,1)}, bf16[128,2,64]{0,2,1:T(8,128)(2,1)}, u32[]{:S(2)}, u32[]{:S(2)}) %collective-permute-start.2) | collective-permute-done | bytes 32800 | tf_op jit(solution)/shard_map/ppermute | solution.py:26
  236.3 2.0 fusion.4
  239.8 6.6 %all-to-all-done.1 = bf16[128,16,1024]{2,1,0:T(8,128)(2,1)} async-done(((bf16[128,16,1024]{2,1,0:T(8,128)(2,1)}), bf16[128,16,1024]{2,1,0:T(8,128)(2,1)}, u32[]{:S(2)}, u32[]{:S(2)}) %all-to-all-start.1) | async-done | bytes 4194336 | tf_op jit(solution)/shard_map/all_to_all | solution.py:55
  246.4 3.0 %fusion.13 = f32[512,2048]{1,0:T(8,128)S(1)} fusion(bf16[2048,1024]{1,0:T(8,128)(2,1)} %bitcast.33, f32[512,512]{1,0:T(8,128)S(1)} %get-tuple-element.4, f32[512]{0:T(512)S(1)} %copy-done.10, f32[512]{0:T(512)S(1)} %get-tuple-element.41, f32[512]{0:T(512)S(1)} %get-tuple-element.40), kind=kOutput, calls=%fused_computation.17 | convolution fusion | flops 1075838976 | bytes 7346176 | tf_op jit(solution)/shard_map/dot_general | solution.py:183
  249.5 2.9 %add_convert_fusion = bf16[512,2048]{1,0:T(8,128)(2,1)S(1)} fusion(f32[512,2048]{1,0:T(8,128)S(1)} %fusion.13, bf16[2048,1024]{1,0:T(8,128)(2,1)} %bitcast.33, bf16[64,8,4,128]{3,2,1,0:T(4,128)(2,1)S(1)} %bitcast.110), kind=kOutput, calls=%fused_computation.12 | convolution fusion | flops 1075838976 | bytes 8912896 | tf_op jit(solution)/shard_map/dot_general | solution.py:184
  252.4 29.1 %all_to_all.16 = bf16[4,128,2048]{2,1,0:T(8,128)(2,1)S(1)} all-to-all(bf16[4,128,2048]{2,1,0:T(8,128)(2,1)S(1)} %bitcast.109), channel_id=1, replica_groups=mesh['sp'=128,'tp'=4] {'tp'}, dimensions={0} | all-to-all | bytes 4194304 | tf_op jit(solution)/shard_map/all_to_all | solution.py:75
  281.6 1.3 reduce_sum.62
  (70 shorter events, 16.3 us)
Async XLA Ops:
  7.2 94.4 %all-gather.2.cloned.1.call-start = ((), (), s32[]{:S(2)}) async-start(), calls=%async_computation.3 | async-start | bytes 7397376 | tf_op jit(solution)/shard_map/all_gather | solution.py:19
  10.8 0.6 copy-start.3
  12.1 138.9 %copy-start.7 = (f32[2048]{0:T(1024)}, f32[2048]{0:T(1024)S(1)}, u32[]{:S(2)}) copy-start(f32[2048]{0:T(1024)S(1)} %convert_element_type.78) | copy-start | bytes 24580
  14.2 136.8 %copy-start.8 = (f32[512]{0:T(512)}, f32[512]{0:T(512)S(1)}, u32[]{:S(2)}) copy-start(f32[512]{0:T(512)S(1)} %add_rsqrt_fusion.1) | copy-start | bytes 6148
  15.4 89.9 %copy-start = (bf16[512,2048]{1,0:T(8,128)(2,1)S(1)}, bf16[512,2048]{1,0:T(8,128)(2,1)}, u32[]{:S(2)}) copy-start(bf16[512,2048]{1,0:T(8,128)(2,1)} %param.12) | copy-start | bytes 6291460
  108.2 6.4 %collective-permute-start = (bf16[30,512]{1,0:T(8,128)(2,1)S(1)}, bf16[30,512]{1,0:T(8,128)(2,1)S(1)}, u32[]{:S(2)}, u32[]{:S(2)}) collective-permute-start(bf16[30,512]{1,0:T(8,128)(2,1)S(1)} %slice.319), channel_id=1, source_target_pairs={{0,4},{4,8},{8,12},{12,16},{16,20},{20,24},{24,28},{28,32},{32,36}... | collective-permute-start | bytes 92168 | tf_op jit(solution)/shard_map/ppermute | solution.py:26
  114.8 10.0 %copy-start.5 = (bf16[512,16]{0,1:T(8,128)(2,1)S(1)}, bf16[512,16]{0,1:T(8,128)(2,1)}, u32[]{:S(2)}) copy-start(bf16[512,16]{0,1:T(8,128)(2,1)} %param.23) | copy-start | bytes 49156
  114.8 9.9 %copy-start.6 = (bf16[512,16]{0,1:T(8,128)(2,1)S(1)}, bf16[512,16]{0,1:T(8,128)(2,1)}, u32[]{:S(2)}) copy-start(bf16[512,16]{0,1:T(8,128)(2,1)} %param.22) | copy-start | bytes 49156
  120.5 9.6 %all-to-all-start = ((f32[4,1,1024]{2,1,0:T(1,128)}), f32[4,1,1024]{2,1,0:T(1,128)S(1)}, u32[]{:S(2)}, u32[]{:S(2)}) async-start(f32[4,1,1024]{2,1,0:T(1,128)} %broadcast_in_dim.14), calls=%async_computation | async-start | bytes 32768 | tf_op jit(solution)/shard_map/all_to_all | solution.py:31
  132.7 11.5 %copy-start.11 = (f32[8]{0:T(128)S(1)}, f32[8]{0:T(128)}, u32[]{:S(2)}) copy-start(f32[8]{0:T(128)} %param.21) | copy-start | bytes 100
  132.7 113.8 %all-to-all-start.1 = ((bf16[128,16,1024]{2,1,0:T(8,128)(2,1)}), bf16[128,16,1024]{2,1,0:T(8,128)(2,1)}, u32[]{:S(2)}, u32[]{:S(2)}) async-start(bf16[128,16,1024]{2,1,0:T(8,128)(2,1)} %stack.2), calls=%async_computation.1 | async-start | bytes 8388608 | tf_op jit(solution)/shard_map/all_to_all | solution.py:55
  148.8 85.8 %collective-permute-start.2 = (bf16[128,2,64]{0,2,1:T(8,128)(2,1)}, bf16[128,2,64]{0,2,1:T(8,128)(2,1)}, u32[]{:S(2)}, u32[]{:S(2)}) collective-permute-start(bf16[128,2,64]{0,2,1:T(8,128)(2,1)} %pad_maximum_fusion.3), channel_id=1, source_target_pairs={{0,4},{4,8},{8,12},{12,16},{16,20},{20,24},{24,28},{28,32},{32,36}... | collective-permute-start | bytes 98312 | tf_op jit(solution)/shard_map/ppermute | solution.py:26
  156.9 0.7 copy-start.1
  158.5 76.9 %collective-permute-start.1 = (bf16[128,2,64]{0,2,1:T(8,128)(2,1)S(1)}, bf16[128,2,64]{0,2,1:T(8,128)(2,1)S(1)}, u32[]{:S(2)}, u32[]{:S(2)}) collective-permute-start(bf16[128,2,64]{0,2,1:T(8,128)(2,1)S(1)} %bitcast.114), channel_id=1, source_target_pairs={{0,4},{4,8},{8,12},{12,16},{16,20},{20,24},{24,28},{28,32},{32,36}... | collective-permute-start | bytes 98312 | tf_op jit(solution)/shard_map/ppermute | solution.py:26
  162.1 76.2 %copy-start.9 = (f32[2,4]{1,0:T(2,128)S(1)}, f32[2,4]{1,0:T(2,128)}, u32[]{:S(2)}) copy-start(f32[2,4]{1,0:T(2,128)} %add.243) | copy-start | bytes 100
  162.1 76.3 %copy-start.2 = (pred[4,128,256]{1,2,0:T(8,128)(4,1)S(1)}, pred[4,128,256]{1,2,0:T(8,128)(4,1)}, u32[]{:S(2)}) copy-start(pred[4,128,256]{1,2,0:T(8,128)(4,1)} %broadcast_and_fusion) | copy-start | bytes 393220
  238.3 8.1 %copy-start.10 = (f32[512]{0:T(512)S(1)}, f32[512]{0:T(512)}, u32[]{:S(2)}) copy-start(f32[512]{0:T(512)} %param.20) | copy-start | bytes 6148
  238.4 11.1 %copy-start.4 = (f32[4,2,4,128]{3,2,1,0:T(4,128)}, f32[4,2,4,128]{3,2,1,0:T(4,128)S(1)}, u32[]{:S(2)}) copy-start(f32[4,2,4,128]{3,2,1,0:T(4,128)S(1)} %add_log_fusion) | copy-start | bytes 49156
Sparse Core Ops, SparseCore 0:
  11.7 89.8 all-gather.1
